TPU v7x, 32 devices: a whole 2x2x4 slice. The times are simulated.
32 devices in a mesh: sp: 8 (over z, y), tp: 4 (over x, core).
Axes of the slice: x: 2, y: 2, z: 4, core: 2. Of those that a mesh axis runs over, the one named last changes fastest.
Arguments:
- queries: bfloat16 [4096, 512], P('sp', 'tp'), may hold values from -6 to 6
- keys: bfloat16 [4096, 512], P('sp', 'tp'), may hold values from -6 to 6
- values: bfloat16 [4096, 1024], P('sp', 'tp'), may hold values from -6 to 6
- input_gate_log: float32 [8, 4096], P('tp', 'sp'), may hold values from -5 to 128
- forget_gate_logits: float32 [8, 4096], P('tp', 'sp'), may hold values from 1 to 16
- extra_decay_log: float32 [8, 4096], P('tp', 'sp'), may hold values from -1 to 0
- output_gate_logits: bfloat16 [4096, 1024], P('sp', 'tp'), may hold values from -6 to 6
- head_norm_scale: float32 [1024], P('tp'), may hold values from 0.1 to 1.9
- layer_residual_input: bfloat16 [4096, 2048], P(('sp', 'tp')), may hold values from -6 to 6
- output_projection_weight: bfloat16 [1024, 2048], replicated, may hold values from -0.1875 to 0.1875
- expert_norm_scale: float32 [2048], replicated, may hold values from 0.1 to 1.9
- routing_expert_index: int32 [4096, 2], P(('sp', 'tp')), may hold values from 0 to 31, all different within a row; in each aligned block of 128 rows (0 to 127, 128 to 255, ...) at most 16 rows name the same one
- routing_expert_weight: float32 [4096, 2], P(('sp', 'tp')), may hold values from 0.2 to 1
- expert_gate_weight: bfloat16 [32, 2048, 1024], P(('sp', 'tp')), may hold values from -0.125 to 0.125
- expert_up_weight: bfloat16 [32, 2048, 1024], P(('sp', 'tp')), may hold values from -0.125 to 0.125
- expert_down_weight: bfloat16 [32, 1024, 2048], P(('sp', 'tp')), may hold values from -0.1875 to 0.1875
Outputs:
- result: bfloat16 [4096, 2048], P(('sp', 'tp'))
Inputs may be any that keep to these rules, and one draw needn't show every extreme that they name: `routing_expert_index`: each row names 2 different experts. Within each aligned block of 128 rows (the rows of one device) no expert is named more than 16 times, a bound that some block reaches in every draw.
All inputs are finite; a program needn't handle non-finite values.
Results may differ from a plain program's by a relative error of at most 0.013.
Values may be sent and summed in bfloat16 or wider, within the bound.
A program may use at most 64 MiB of HBM per device.

v0:
```python
import functools

import jax
import jax.numpy as jnp
from jax import lax
from jax.experimental import pallas as pl
from jax.experimental.pallas import tpu as pltpu
from jax.sharding import PartitionSpec as P

TOP = 2
BLOCK = 128


very_low = -1e30
epsilon = 1e-06
highest = lax.Precision.HIGHEST
MESH = pl.DeviceIdType.MESH


def join_kernel(n, heads, key_width, memory_ref, scalars_ref, out_memory, out_scalars,
                got_memory, got_scalars, send_memory, send_scalars, recv_memory, recv_scalars):
    me = lax.axis_index("sp")
    barrier = pltpu.get_barrier_semaphore()
    for k in range(1, n):
        other = lax.rem(me + k, n)
        pl.semaphore_signal(barrier, inc=1, device_id={"sp": other}, device_id_type=MESH)
    pl.semaphore_wait(barrier, n - 1)

    def copies(source, target):
        kind = dict(device_id={"sp": target}, device_id_type=MESH)
        return (
            pltpu.make_async_remote_copy(
                src_ref=memory_ref, dst_ref=got_memory.at[source],
                send_sem=send_memory.at[target], recv_sem=recv_memory.at[source], **kind),
            pltpu.make_async_remote_copy(
                src_ref=scalars_ref, dst_ref=got_scalars.at[source],
                send_sem=send_scalars.at[target], recv_sem=recv_scalars.at[source], **kind),
        )

    for k in range(n - 1, 0, -1):
        @pl.when(me + k < n)
        def _(k=k):
            for copy in copies(me, me + k):
                copy.start()

    out_memory[...] = jnp.zeros_like(out_memory)
    out_scalars[...] = jnp.full_like(out_scalars, very_low)

    def lap(j, carry):
        for copy in copies(j, me):
            copy.wait_recv()
        for h in range(heads):
            decay = got_scalars[j, h : h + 1, :]
            stab_late = got_scalars[j, heads + h : heads + h + 1, :]
            shifted = decay + out_scalars[h : h + 1, :]
            combined = jnp.maximum(shifted, stab_late)
            rows = slice(h * key_width, (h + 1) * key_width)
            out_memory[rows, :] = jnp.exp(shifted - combined) * out_memory[rows, :] + jnp.exp(
                stab_late - combined
            ) * got_memory[j, rows, :].astype(jnp.float32)
            out_scalars[h : h + 1, :] = combined
        return carry

    lax.fori_loop(0, me, lap, 0)
    for k in range(1, n):
        @pl.when(me + k < n)
        def _(k=k):
            for copy in copies(me, me + k):
                copy.wait_send()


def incoming_state(decay, memory, stabilizer):
    heads, key_width, value_width = memory.shape
    n = lax.axis_size("sp")
    scalar_rows = -(-2 * heads // 8) * 8
    scalars = jnp.concatenate(
        [decay, stabilizer, jnp.zeros((scalar_rows - 2 * heads,), jnp.float32)]
    )
    scalars = jnp.broadcast_to(scalars[:, None], (scalar_rows, value_width))
    flat = memory.reshape(heads * key_width, value_width).astype(jnp.bfloat16)
    vmem = pl.BlockSpec(memory_space=pltpu.VMEM)
    out_memory, out_scalars = pl.pallas_call(
        functools.partial(join_kernel, n, heads, key_width),
        out_shape=(
            jax.ShapeDtypeStruct(flat.shape, jnp.float32),
            jax.ShapeDtypeStruct(scalars.shape, jnp.float32),
        ),
        in_specs=[vmem, vmem],
        out_specs=(vmem, vmem),
        scratch_shapes=[
            pltpu.VMEM((n,) + flat.shape, jnp.bfloat16),
            pltpu.VMEM((n,) + scalars.shape, jnp.float32),
        ]
        + [pltpu.SemaphoreType.DMA((n,))] * 4,
        compiler_params=pltpu.CompilerParams(collective_id=0, has_side_effects=True),
    )(flat, scalars)
    return out_memory.reshape(memory.shape), out_scalars[:heads, 0]


def all_blocks(query_blk, key_blk, value_blk, input_blk, forget_blk):
    blocks, heads, length = forget_blk.shape
    within = jnp.cumsum(forget_blk, axis=-1)
    causal = jnp.arange(length)[:, None] >= jnp.arange(length)[None, :]
    log_weight = jnp.where(
        causal, within[..., :, None] - within[..., None, :] + input_blk[..., None, :], very_low
    )
    largest = jnp.max(log_weight, axis=-1)
    intra_weight = jnp.exp(log_weight - largest[..., None])
    scores = jnp.einsum("bhtd,bhsd->bhts", query_blk, key_blk, precision=highest) * intra_weight
    numerator = jnp.einsum("bhts,bhsv->bhtv", scores, value_blk, precision=highest)
    block_total = within[..., -1]
    to_end = block_total[..., None] - within + input_blk
    block_max = jnp.max(to_end, axis=-1)
    state_add = jnp.exp(to_end - block_max[..., None])
    block_memory = jnp.einsum(
        "bhsd,bhsv->bhdv", key_blk * state_add[..., None], value_blk, precision=highest
    )
    before = [jnp.zeros((heads,), jnp.float32)]
    memories = [jnp.zeros(block_memory.shape[1:], jnp.float32)]
    maxima = [jnp.full((heads,), very_low, jnp.float32)]
    for b in range(blocks):
        shifted = maxima[b] + block_total[b]
        combined = jnp.maximum(shifted, block_max[b])
        memories.append(
            jnp.exp(shifted - combined)[:, None, None] * memories[b]
            + jnp.exp(block_max[b] - combined)[:, None, None] * block_memory[b]
        )
        maxima.append(combined)
        before.append(before[b] + block_total[b])
    return (numerator, largest, within), (before, memories, maxima)


def expert_kernel(peers, count, members, tile,
                  sent_ref, gate_ref, up_ref, down_ref, high_ref, low_ref, middle_ref, out_ref,
                  arrived, produced, returned, activation, gate_w, up_w, down_w,
                  send_there, recv_there, send_back, recv_back, weight_sems):
    sp = lax.axis_index("sp")
    me = sp * peers + lax.axis_index("tp")
    groups = count // members
    own_group = me // members
    slots, width = sent_ref.shape[1:]
    hidden = gate_w.shape[1]

    def place(device):
        return dict(
            device_id={"sp": device // peers, "tp": lax.rem(device, peers)}, device_id_type=MESH
        )

    weight_copies = [
        pltpu.make_async_copy(source.at[0], target, weight_sems.at[k])
        for k, (source, target) in enumerate(
            ((gate_ref, gate_w), (up_ref, up_w), (down_ref, down_w))
        )
    ]
    for copy in weight_copies:
        copy.start()

    def there(source, target):
        return pltpu.make_async_remote_copy(
            src_ref=sent_ref.at[target], dst_ref=arrived.at[source],
            send_sem=send_there.at[target], recv_sem=recv_there.at[source], **place(target))

    def back(source, target):
        return pltpu.make_async_remote_copy(
            src_ref=produced.at[target], dst_ref=returned.at[source],
            send_sem=send_back.at[target], recv_sem=recv_back.at[source], **place(target))

    barrier = pltpu.get_barrier_semaphore()

    def greet(k, carry):
        pl.semaphore_signal(barrier, inc=1, **place(lax.rem(me + k, count)))
        return carry

    lax.fori_loop(1, count, greet, 0)
    pl.semaphore_wait(barrier, count - 1)

    def group_of(step):
        return lax.rem(own_group + lax.rem(step, 2) * (groups // 2) + step // 2, groups)

    def dispatch(index, carry):
        target = group_of(lax.rem(index // members + 1, groups)) * members + lax.rem(index, members)

        @pl.when(target != me)
        def _():
            there(me, target).start()

        return carry

    lax.fori_loop(0, count, dispatch, 0)
    arrived[me] = sent_ref[me]
    for copy in weight_copies:
        copy.wait()

    def one_group(step, carry):
        first = group_of(step) * members

        def receive(j, carry):
            @pl.when(first + j != me)
            def _():
                there(first + j, me).wait_recv()

            return carry

        lax.fori_loop(0, members, receive, 0)

        def hidden_tile(t, carry):
            columns = pl.ds(pl.multiple_of(t * tile, tile), tile)
            rows = arrived[pl.ds(first, members)].reshape(members * slots, width)
            gate_part = jnp.dot(rows, gate_w[:, columns], preferred_element_type=jnp.float32)
            up_part = jnp.dot(rows, up_w[:, columns], preferred_element_type=jnp.float32)
            activation[:, columns] = (jax.nn.silu(gate_part) * up_part).astype(jnp.bfloat16)
            return carry

        lax.fori_loop(0, hidden // tile, hidden_tile, 0)

        def width_tile(t, carry):
            columns = pl.ds(pl.multiple_of(t * tile, tile), tile)
            part = jnp.dot(
                activation[...], down_w[:, columns], preferred_element_type=jnp.float32
            ).astype(jnp.bfloat16)
            produced[pl.ds(first, members), :, columns] = part.reshape(members, slots, tile)
            return carry

        lax.fori_loop(0, width // tile, width_tile, 0)

        def give_back(j, carry):
            @pl.when(first + j != me)
            def _():
                back(me, first + j).start()

            return carry

        lax.fori_loop(0, members, give_back, 0)
        return carry

    lax.fori_loop(0, groups, one_group, 0)
    returned[me] = produced[me]

    def collect(k, carry):
        back(lax.rem(me + k, count), me).wait_recv()
        return carry

    lax.fori_loop(1, count, collect, 0)

    def combine_tile(t, carry):
        columns = pl.ds(pl.multiple_of(t * tile, tile), tile)
        rows = returned[:, :, columns].reshape(count * slots, tile)
        total = jnp.dot(high_ref[...], rows, preferred_element_type=jnp.float32) + jnp.dot(
            low_ref[...], rows, preferred_element_type=jnp.float32
        )
        out_ref[:, columns] = (middle_ref[:, columns].astype(jnp.float32) + total).astype(
            jnp.bfloat16
        )
        return carry

    lax.fori_loop(0, width // tile, combine_tile, 0)

    def finish(k, carry):
        target = lax.rem(me + k, count)
        there(me, target).wait_send()
        back(me, target).wait_send()
        return carry

    lax.fori_loop(1, count, finish, 0)


def expert_call(sent, gate, up, down, high, low, middle):
    count, slots, width = sent.shape
    hidden = gate.shape[2]
    peers = lax.axis_size("tp")
    vmem = pl.BlockSpec(memory_space=pltpu.VMEM)
    anywhere = pl.BlockSpec(memory_space=pl.ANY)
    members = count // 4
    return pl.pallas_call(
        functools.partial(expert_kernel, peers, count, members, 256),
        out_shape=jax.ShapeDtypeStruct(middle.shape, jnp.bfloat16),
        in_specs=[vmem, anywhere, anywhere, anywhere, vmem, vmem, vmem],
        out_specs=vmem,
        scratch_shapes=[
            pltpu.VMEM(sent.shape, jnp.bfloat16),
            pltpu.VMEM(sent.shape, jnp.bfloat16),
            pltpu.VMEM(sent.shape, jnp.bfloat16),
            pltpu.VMEM((members * slots, hidden), jnp.bfloat16),
            pltpu.VMEM((width, hidden), jnp.bfloat16),
            pltpu.VMEM((width, hidden), jnp.bfloat16),
            pltpu.VMEM((hidden, width), jnp.bfloat16),
        ]
        + [pltpu.SemaphoreType.DMA((count,))] * 4
        + [pltpu.SemaphoreType.DMA((3,))],
        compiler_params=pltpu.CompilerParams(collective_id=1, has_side_effects=True),
    )(sent, gate, up, down, high, low, middle)


def shards(
    queries,
    keys,
    values,
    input_gate_log,
    forget_gate_logits,
    extra_decay_log,
    output_gate_logits,
    head_norm_scale,
    layer_residual_input,
    output_projection_weight,
    expert_norm_scale,
    routing_expert_index,
    routing_expert_weight,
    expert_gate_weight,
    expert_up_weight,
    expert_down_weight,
):
    positions = queries.shape[0]
    heads_here = input_gate_log.shape[0]
    key_width = queries.shape[1] // heads_here
    value_width = values.shape[1] // heads_here
    blocks = positions // BLOCK

    def to_blocks(matrix, columns):
        return (
            matrix.astype(jnp.float32)
            .reshape(blocks, BLOCK, heads_here, columns)
            .transpose(0, 2, 1, 3)
        )

    def gate_blocks(matrix):
        return matrix.reshape(heads_here, blocks, BLOCK).transpose(1, 0, 2)

    query_blocks = to_blocks(queries, key_width) * key_width ** (-0.5)
    key_blocks = to_blocks(keys, key_width)
    value_blocks = to_blocks(values, value_width)
    forget_log_value = jax.nn.log_sigmoid(forget_gate_logits) + extra_decay_log
    sequence_inputs = (
        query_blocks,
        key_blocks,
        value_blocks,
        gate_blocks(input_gate_log),
        gate_blocks(forget_log_value),
    )
    (numerator, largest, within), (before, memories, maxima) = all_blocks(*sequence_inputs)
    earlier_memory, earlier_max = incoming_state(before[-1], memories[-1], maxima[-1])
    local_max = jnp.stack(maxima[:-1])
    moved_max = jnp.stack(before[:-1]) + earlier_max[None, :]
    start_max = jnp.maximum(moved_max, local_max)
    start_memory = (
        jnp.exp(moved_max - start_max)[..., None, None] * earlier_memory[None]
        + jnp.exp(local_max - start_max)[..., None, None] * jnp.stack(memories[:-1])
    )
    from_start = within + start_max[..., None]
    combined = jnp.maximum(largest, from_start)
    old_part = jnp.exp(largest - combined)
    new_part = jnp.exp(from_start - combined)
    numerator = old_part[..., None] * numerator + new_part[..., None] * jnp.einsum(
        "bhtd,bhdv->bhtv", query_blocks, start_memory, precision=highest
    )
    cell_out = numerator.transpose(0, 2, 1, 3).reshape(positions, heads_here, value_width)
    scaled = cell_out * lax.rsqrt(jnp.mean(cell_out * cell_out, axis=-1, keepdims=True) + epsilon)
    gated_out = (
        jax.nn.sigmoid(output_gate_logits.astype(jnp.float32)).reshape(
            positions, heads_here, value_width
        )
        * scaled
        * head_norm_scale.reshape(heads_here, value_width)
    )
    mixture = gated_out.reshape(positions, heads_here * value_width).astype(jnp.bfloat16)
    token_mix = lax.all_to_all(mixture, "tp", split_axis=0, concat_axis=1, tiled=True)
    projected = jnp.dot(token_mix, output_projection_weight, preferred_element_type=jnp.float32)
    middle = (layer_residual_input.astype(jnp.float32) + projected).astype(jnp.bfloat16)
    middle_wide = middle.astype(jnp.float32)
    normed = (
        middle_wide
        * lax.rsqrt(jnp.mean(middle_wide * middle_wide, axis=-1, keepdims=True) + epsilon)
        * expert_norm_scale
    ).astype(jnp.bfloat16)
    tok_count = normed.shape[0]
    model_width = normed.shape[1]
    sp_count = lax.axis_size("sp")
    tp_count = lax.axis_size("tp")
    devices = sp_count * tp_count
    local_experts = expert_gate_weight.shape[0]
    experts = local_experts * devices
    slots = max(2, 2 * tok_count * TOP // experts)
    entries = tok_count * TOP
    flat_ids = routing_expert_index.reshape(-1)
    one_hot = (flat_ids[:, None] == jnp.arange(experts, dtype=jnp.int32)[None, :]).astype(
        jnp.bfloat16
    )
    earlier_rows = (jnp.arange(entries)[:, None] > jnp.arange(entries)[None, :]).astype(
        jnp.bfloat16
    )
    seen_before = jnp.dot(earlier_rows, one_hot, preferred_element_type=jnp.float32)
    position_in = jnp.sum(seen_before * one_hot.astype(jnp.float32), axis=1).astype(jnp.int32)
    slot_key = flat_ids * slots + position_in
    matches = slot_key[None, :] == jnp.arange(experts * slots, dtype=jnp.int32)[:, None]
    pick = jnp.sum(
        matches.reshape(experts * slots, tok_count, TOP).astype(jnp.float32), axis=2
    ).astype(jnp.bfloat16)
    outgoing = (
        jnp.dot(pick, normed, preferred_element_type=jnp.float32)
        .astype(jnp.bfloat16)
        .reshape(experts, slots, model_width)
    )
    weight_high = lax.reduce_precision(routing_expert_weight, 8, 7)
    slot_pairs = slot_key.reshape(tok_count, TOP, 1)
    slot_range = jnp.arange(experts * slots, dtype=jnp.int32)

    def spread(weights):
        return jnp.sum(
            jnp.where(slot_pairs == slot_range, weights[:, :, None], 0.0), axis=1
        ).astype(jnp.bfloat16)

    high = spread(weight_high)
    low = spread(routing_expert_weight - weight_high)
    if local_experts == 1 and slots % 16 == 0 and devices % 4 == 0:
        return expert_call(
            outgoing, expert_gate_weight, expert_up_weight, expert_down_weight, high, low, middle
        )
    arrived = lax.all_to_all(outgoing, ("sp", "tp"), split_axis=0, concat_axis=0, tiled=True)
    grouped = arrived.reshape(devices, local_experts, arrived.shape[1], model_width)
    gate_part = jnp.einsum(
        "sxcd,xdf->sxcf", grouped, expert_gate_weight, preferred_element_type=jnp.float32
    )
    up_part = jnp.einsum(
        "sxcd,xdf->sxcf", grouped, expert_up_weight, preferred_element_type=jnp.float32
    )
    activation = (jax.nn.silu(gate_part) * up_part).astype(jnp.bfloat16)
    produced = jnp.einsum(
        "sxcf,xfd->sxcd", activation, expert_down_weight, preferred_element_type=jnp.float32
    ).astype(jnp.bfloat16)
    returned = lax.all_to_all(
        produced.reshape(arrived.shape), ("sp", "tp"), split_axis=0, concat_axis=0, tiled=True
    )
    returned = returned.reshape(experts * slots, model_width)
    expert_sum = jnp.dot(high, returned, preferred_element_type=jnp.float32) + jnp.dot(
        low, returned, preferred_element_type=jnp.float32
    )
    return (middle_wide + expert_sum).astype(jnp.bfloat16)


def solution(mesh):
    in_specs = (
        P("sp", "tp"),
        P("sp", "tp"),
        P("sp", "tp"),
        P("tp", "sp"),
        P("tp", "sp"),
        P("tp", "sp"),
        P("sp", "tp"),
        P("tp"),
        P(("sp", "tp"), None),
        P(),
        P(),
        P(("sp", "tp"), None),
        P(("sp", "tp"), None),
        P(("sp", "tp"), None, None),
        P(("sp", "tp"), None, None),
        P(("sp", "tp"), None, None),
    )
    out_specs = P(("sp", "tp"), None)
    return jax.shard_map(shards, mesh=mesh, in_specs=in_specs, out_specs=out_specs, check_vma=False)
```

profile of v0, /device:TPU:7, one launch (start us, length us, event | category | flops | bytes accessed | tf_op | source)
XLA Modules:
  0.0 151.5 jit_solution(877607853484950319)
XLA Ops:
  0.0 0.7 fusion.49
  0.7 1.2 reduce_window_sum.11
  2.0 0.2 slice_reduce_fusion.3
  2.5 0.8 fusion.66
  3.4 0.8 subtract_exponential_fusion
  5.4 1.0 copy.109
  6.5 0.9 convert_multiply_fusion.2
  7.7 1.0 reshape.552
  8.7 0.2 copy.123
  8.9 0.6 fusion.23
  9.7 0.8 fusion.36.memory_ref
  10.6 0.7 broadcast_in_dim.29.scalars_ref
  11.2 9.2 %shard_map.154 = (f32[128,128]{1,0:T(8,128)}, f32[8,128]{1,0:T(8,128)}) custom-call(bf16[128,128]{1,0:T(8,128)(2,1)} %fusion.36.memory_ref, f32[8,128]{1,0:T(8,128)} %broadcast_in_dim.29.scalars_ref), custom_call_target="tpu_custom_call" | custom-call | tf_op jit(solution)/shard_map/pallas_call | solution.py:82
  20.4 0.8 slice_reduce_fusion.1
  21.2 0.4 fusion.14
  21.9 0.8 convolution_multiply_fusion
  22.7 0.7 fusion.3
  23.4 1.9 %multiply_reduce_fusion = (f32[4,128,2]{1,2,0:T(2,128)S(1)}, f32[4,128,2,128]{1,3,2,0:T(8,128)S(1)}) fusion(f32[4,128,2,128]{1,3,2,0:T(8,128)S(1)} %fusion.3, f32[1,2,64,128]{3,2,1,0:T(8,128)S(1)} %get-tuple-element.19, f32[1,2,64,128]{3,2,1,0:T(8,128)S(1)} %get-tuple-element.20, f32[1,2,64,128]{3,2,1,0:T(8,128)S(1)} %get-tuple-element.21, ...), kind=kOutput, calls=%fused_computation.25 | convolution fusion | flops 101579776 | bytes 1581136 | tf_op jit(solution)/shard_map/bhtd,bhdv->bhtv/dot_general | solution.py:352
  25.4 0.2 copy.119
  25.5 0.3 copy.118
  25.8 0.6 mul.325
  26.4 0.2 fusion.11
  26.6 0.8 copy.120
  27.4 5.0 %all-to-all-start = ((bf16[4,128,256]{1,2,0:T(8,128)(2,1)}), bf16[4,128,256]{1,2,0:T(8,128)(2,1)S(1)}, u32[]{:S(2)}, u32[]{:S(2)}) async-start(bf16[4,128,256]{1,2,0:T(8,128)(2,1)} %copy.120), calls=%async_computation | async-start | bytes 524288 | tf_op jit(solution)/shard_map/all_to_all | solution.py:365
  32.6 0.1 eq.21
  32.7 0.2 fusion.4
  33.2 0.9 select_reduce_fusion
  34.1 2.5 %all-to-all-done = bf16[4,128,256]{1,2,0:T(8,128)(2,1)S(1)} async-done(((bf16[4,128,256]{1,2,0:T(8,128)(2,1)}), bf16[4,128,256]{1,2,0:T(8,128)(2,1)S(1)}, u32[]{:S(2)}, u32[]{:S(2)}) %all-to-all-start) | async-done | bytes 262176 | tf_op jit(solution)/shard_map/all_to_all | solution.py:365
  36.6 3.0 %fusion.5 = (f32[128]{0:T(128)S(1)}, bf16[128,2048]{1,0:T(8,128)(2,1)S(1)}) fusion(bf16[128,1024]{0,1:T(8,128)(2,1)S(1)} %bitcast.162, bf16[1024,2048]{1,0:T(8,128)(2,1)} %param.25, bf16[128,2048]{1,0:T(8,128)(2,1)S(1)} %copy-done.1), kind=kOutput, calls=%fused_computation.13 | convolution fusion | flops 538443648 | bytes 5505536 | tf_op jit(solution)/shard_map/dot_general | solution.py:366
  39.7 2.2 %convolution_convert_fusion = bf16[512,2048]{1,0:T(8,128)(2,1)} fusion(bf16[128,2048]{1,0:T(8,128)(2,1)S(1)} %get-tuple-element.56.middle_ref, f32[2048]{0:T(1024)S(1)} %copy-done.4, f32[128]{0:T(128)S(1)} %add_rsqrt_fusion, bf16[512,128]{1,0:T(8,128)(2,1)S(1)} %convert_reduce_fusion), kind=kOutput, calls=%fused_computation | convolution fusion | flops 270532608 | bytes 2761216 | tf_op jit(solution)/shard_map/dot_general | solution.py:398
  41.8 107.8 %shard_map.155 = bf16[128,2048]{1,0:T(8,128)(2,1)} custom-call(bf16[32,16,2048]{2,1,0:T(8,128)(2,1)} %bitcast.159, bf16[1,2048,1024]{2,1,0:T(8,128)(2,1)} %gate_ref.1, bf16[1,2048,1024]{2,1,0:T(8,128)(2,1)} %up_ref.1, bf16[1,1024,2048]{2,1,0:T(8,128)(2,1)} %down_ref.1, bf16[128,512]{1,0:T(8,128)(2,1)} %get-tuple-element.16.high_ref, ...), custom_call_target="tpu_custom_call" | custom-call | tf_op jit(solution)/shard_map/pallas_call | solution.py:274
  149.6 1.9 %copy.139 = bf16[128,2048]{1,0:T(8,128)(2,1)} copy(bf16[128,2048]{1,0:T(8,128)(2,1)} %shard_map.155) | data formatting | bytes 1048576
  (61 shorter events, 2.8 us)
Async XLA Ops:
  0.0 21.2 %copy-start.3 = (f32[2,512]{1,0:T(2,128)S(1)}, f32[2,512]{1,0:T(2,128)}, u32[]{:S(2)}) copy-start(f32[2,512]{1,0:T(2,128)} %param.19) | copy-start | bytes 12292
  8.9 17.5 %copy-start.2 = (bf16[512,256]{1,0:T(8,128)(2,1)S(1)}, bf16[512,256]{1,0:T(8,128)(2,1)}, u32[]{:S(2)}) copy-start(bf16[512,256]{1,0:T(8,128)(2,1)} %param.22) | copy-start | bytes 786436
  8.9 17.5 %copy-start.7 = (f32[256]{0:T(256)S(1)}, f32[256]{0:T(256)}, u32[]{:S(2)}) copy-start(f32[256]{0:T(256)} %param.23) | copy-start | bytes 3076
  21.9 10.5 %copy-start.6 = (f32[128,2]{0,1:T(2,128)S(1)}, f32[128,2]{0,1:T(2,128)}, u32[]{:S(2)}) copy-start(f32[128,2]{0,1:T(2,128)} %param.28) | copy-start | bytes 3076
  21.9 10.5 %copy-start.5 = (s32[128,2]{0,1:T(2,128)S(1)}, s32[128,2]{0,1:T(2,128)}, u32[]{:S(2)}) copy-start(s32[128,2]{0,1:T(2,128)} %param.27) | copy-start | bytes 3076
  22.7 13.9 %copy-start.1 = (bf16[128,2048]{1,0:T(8,128)(2,1)S(1)}, bf16[128,2048]{1,0:T(8,128)(2,1)}, u32[]{:S(2)}) copy-start(bf16[128,2048]{1,0:T(8,128)(2,1)} %param.24) | copy-start | bytes 1572868
  26.4 13.3 %copy-start.4 = (f32[2048]{0:T(1024)S(1)}, f32[2048]{0:T(1024)}, u32[]{:S(2)}) copy-start(f32[2048]{0:T(1024)} %param.26) | copy-start | bytes 24580
  27.4 9.2 %all-to-all-start = ((bf16[4,128,256]{1,2,0:T(8,128)(2,1)}), bf16[4,128,256]{1,2,0:T(8,128)(2,1)S(1)}, u32[]{:S(2)}, u32[]{:S(2)}) async-start(bf16[4,128,256]{1,2,0:T(8,128)(2,1)} %copy.120), calls=%async_computation | async-start | bytes 524288 | tf_op jit(solution)/shard_map/all_to_all | solution.py:365
  39.6 2.2 %copy-start = (bf16[128,2048]{1,0:T(8,128)(2,1)}, bf16[128,2048]{1,0:T(8,128)(2,1)S(1)}, u32[]{:S(2)}) copy-start(bf16[128,2048]{1,0:T(8,128)(2,1)S(1)} %get-tuple-element.56.middle_ref) | copy-start | bytes 1572868
where the time goes:
time: 152 us; the launch traced here: 151 us
  Pallas kernels  117 us (77%)
  local copies, waits for them, and re-layouts  9.64 us (6%)
  matrix products  9.38 us (6%)
  other arithmetic  7.66 us (5%)
  starting transfers between devices  5.01 us (3%)
  waiting for transfers between devices  2.48 us (2%)
    pallas_call x1, Pallas kernels, expert_call(): pl.pallas_call(functools.partial(expert_kernel, peers, count, members, 25...  108 us
    pallas_call x1, Pallas kernels, incoming_state(): pl.pallas_call(functools.partial(join_kernel, n, heads, key_width), out_s...  9.2 us
    all_to_all x1, starting transfers between devices, shards(): lax.all_to_all(mixture, 'tp', split_axis=0, concat_axis=1, tiled=True)  5.01 us
    unnamed x19, local copies, waits for them, and re-layouts  3.05 us
  transfers between devices with their start and end apart: 1, of which 1 were waited for; matrix products, arithmetic and copies ran while one was open for 1% of the time, Pallas kernels for 0%

commit v1 on v0

v1 whole, which is shorter than its diff:
```python
import functools

import jax
import jax.numpy as jnp
from jax import lax
from jax.experimental import pallas as pl
from jax.experimental.pallas import tpu as pltpu
from jax.sharding import PartitionSpec as P

TOP = 2
BLOCK = 128
PLANES = 4


very_low = -1e30
epsilon = 1e-06
MESH = pl.DeviceIdType.MESH


def split(value):
    high = value.astype(jnp.bfloat16)
    return high, (value - high.astype(jnp.float32)).astype(jnp.bfloat16)


def dot_f32(a, b):
    return jnp.dot(a, b, preferred_element_type=jnp.float32)


def along_lanes(value, join, empty):
    lane = lax.broadcasted_iota(jnp.int32, value.shape, 1)
    shift = 1
    while shift < value.shape[1]:
        moved = jnp.where(lane >= shift, pltpu.roll(value, shift, 1), empty)
        value = join(value, moved)
        shift *= 2
    return value


def route_notes(index_ref, weight_ref, experts, slots):
    tokens = index_ref.shape[1]
    expert = lax.broadcasted_iota(jnp.int32, (experts, tokens), 0)
    before = lax.broadcasted_iota(jnp.int32, (tokens, tokens), 0) < lax.broadcasted_iota(
        jnp.int32, (tokens, tokens), 1
    )
    before = jnp.where(before, 1.0, 0.0).astype(jnp.bfloat16)
    base = jnp.zeros((experts, 1), jnp.float32)
    lines = []
    for j in range(TOP):
        row = index_ref[j : j + 1, :]
        named = jnp.where(expert == row, 1.0, 0.0)
        seen = dot_f32(named.astype(jnp.bfloat16), before) + base
        position = jnp.sum(named * seen, axis=0, keepdims=True)
        lines.append(row.astype(jnp.float32) * slots + position)
        base = base + jnp.sum(named, axis=1, keepdims=True)
    lines += [weight_ref[j : j + 1, :] for j in range(TOP)]
    lines.append(jnp.zeros((8 - 2 * TOP, tokens), jnp.float32))
    return jnp.concatenate(lines, axis=0)


def cell_kernel(n, tp_size, heads, experts, slots,
                query_ref, key_ref, value_ref, input_ref, forget_ref, extra_ref, gate_ref,
                head_scale_ref, residual_ref, projection_ref, norm_scale_ref, index_ref, weight_ref,
                middle_ref, normed_ref, notes_ref,
                state, state_notes, got_state, got_notes, carried, intra, mix, token_mix, weights,
                send_state, send_notes, recv_state, recv_notes, send_mix, recv_mix, weight_sem):
    sp = lax.axis_index("sp")
    tp = lax.axis_index("tp")
    length = query_ref.shape[0]
    blocks = length // BLOCK
    keys = query_ref.shape[1] // heads
    wide = value_ref.shape[1] // heads
    share = length // tp_size
    columns = heads * wide

    weight_copy = pltpu.make_async_copy(projection_ref, weights, weight_sem)
    weight_copy.start()
    barrier = pltpu.get_barrier_semaphore()

    def greet_sp(k, carry):
        pl.semaphore_signal(
            barrier, inc=1, device_id={"sp": lax.rem(sp + k, n)}, device_id_type=MESH
        )
        return carry

    lax.fori_loop(1, n, greet_sp, 0)
    for k in range(1, tp_size):
        pl.semaphore_signal(
            barrier, inc=1, device_id={"tp": lax.rem(tp + k, tp_size)}, device_id_type=MESH
        )

    def state_copies(source, target):
        kind = dict(device_id={"sp": target}, device_id_type=MESH)
        return (
            pltpu.make_async_remote_copy(
                src_ref=state, dst_ref=got_state.at[source],
                send_sem=send_state.at[target], recv_sem=recv_state.at[source], **kind),
            pltpu.make_async_remote_copy(
                src_ref=state_notes, dst_ref=got_notes.at[source],
                send_sem=send_notes.at[target], recv_sem=recv_notes.at[source], **kind),
        )

    def mix_copy(source, target):
        return pltpu.make_async_remote_copy(
            src_ref=mix.at[pl.ds(target * share, share), :],
            dst_ref=token_mix.at[:, pl.ds(pl.multiple_of(source * columns, columns), columns)],
            send_sem=send_mix.at[target], recv_sem=recv_mix.at[source],
            device_id={"tp": target}, device_id_type=MESH)

    def by_block(value):
        return jnp.concatenate(
            [value[h : h + 1, b * BLOCK : (b + 1) * BLOCK]
             for h in range(heads) for b in range(blocks)], axis=0)

    logits = forget_ref[...]
    decay = jnp.minimum(logits, 0.0) - jnp.log1p(jnp.exp(-jnp.abs(logits))) + extra_ref[...]
    within = along_lanes(by_block(decay), jnp.add, 0.0)
    level = by_block(input_ref[...]) - within
    peak = along_lanes(level, jnp.maximum, very_low)
    total = within[:, BLOCK - 1 : BLOCK]
    top = peak[:, BLOCK - 1 : BLOCK]
    state_add = jnp.exp(level - top)
    block_max = total + top
    largest = within + peak

    keys_t = key_ref[...].astype(jnp.float32).T
    keys_t_low = keys_t.astype(jnp.bfloat16)
    zero = jnp.zeros((1, 1), jnp.float32)
    state_notes[...] = jnp.zeros_like(state_notes)
    local_max, local_before = [], []
    for h in range(heads):
        memory = jnp.zeros((keys, wide), jnp.float32)
        high_mark = jnp.full((1, 1), very_low, jnp.float32)
        passed = zero
        for b in range(blocks):
            row = h * blocks + b
            carried[row] = memory
            local_max.append(high_mark)
            local_before.append(passed)
            added_high, added_low = split(
                keys_t[h * keys : (h + 1) * keys, b * BLOCK : (b + 1) * BLOCK]
                * state_add[row : row + 1, :]
            )
            values = value_ref[b * BLOCK : (b + 1) * BLOCK, h * wide : (h + 1) * wide]
            added = dot_f32(added_high, values) + dot_f32(added_low, values)
            shifted = high_mark + total[row : row + 1]
            combined = jnp.maximum(shifted, block_max[row : row + 1])
            memory = jnp.exp(shifted - combined) * memory + jnp.exp(
                block_max[row : row + 1] - combined
            ) * added
            high_mark = combined
            passed = passed + total[row : row + 1]
        state[h * keys : (h + 1) * keys, :] = memory.astype(jnp.bfloat16)
        state_notes[h : h + 1, :] = jnp.broadcast_to(passed, (1, wide))
        state_notes[heads + h : heads + h + 1, :] = jnp.broadcast_to(high_mark, (1, wide))
    pl.semaphore_wait(barrier, n + tp_size - 2)

    def send_on(k, carry):
        @pl.when(sp + k < n)
        def _():
            for copy in state_copies(sp, sp + k):
                copy.start()

        return carry

    lax.fori_loop(1, n, send_on, 0)

    notes_ref[...] = route_notes(index_ref, weight_ref, experts, slots)
    causal = lax.broadcasted_iota(jnp.int32, (BLOCK, BLOCK), 0) >= lax.broadcasted_iota(
        jnp.int32, (BLOCK, BLOCK), 1
    )
    lane = lax.broadcasted_iota(jnp.int32, (BLOCK, heads * keys), 1)
    peak_t = peak.T

    def own_query(h, b):
        query = query_ref[b * BLOCK : (b + 1) * BLOCK, :] * jnp.bfloat16(keys ** -0.5)
        return jnp.where(
            (lane >= h * keys) & (lane < (h + 1) * keys), query, jnp.zeros_like(query)
        )

    for h in range(heads):
        for b in range(blocks):
            row = h * blocks + b
            scores = dot_f32(own_query(h, b), keys_t_low[:, b * BLOCK : (b + 1) * BLOCK])
            weight = jnp.exp(
                jnp.where(causal, level[row : row + 1, :] - peak_t[:, row : row + 1], very_low)
            )
            score_high, score_low = split(scores * weight)
            values = value_ref[b * BLOCK : (b + 1) * BLOCK, h * wide : (h + 1) * wide]
            intra[row] = dot_f32(score_high, values) + dot_f32(score_low, values)

    def lap(j, carry):
        memory, marks = carry
        for copy in state_copies(j, sp):
            copy.wait_recv()
        memories, later = [], []
        for h in range(heads):
            passed = got_notes[j, h : h + 1, :]
            late = got_notes[j, heads + h : heads + h + 1, :]
            shifted = passed + marks[h : h + 1, :]
            combined = jnp.maximum(shifted, late)
            memories.append(
                jnp.exp(shifted - combined) * memory[h * keys : (h + 1) * keys, :]
                + jnp.exp(late - combined)
                * got_state[j, h * keys : (h + 1) * keys, :].astype(jnp.float32)
            )
            later.append(combined)
        return jnp.concatenate(memories, axis=0), jnp.concatenate(later, axis=0)

    earlier, marks = lax.fori_loop(
        0, sp, lap,
        (jnp.zeros((heads * keys, wide), jnp.float32), jnp.zeros((heads, wide), jnp.float32)),
    )

    local_marks = jnp.concatenate(local_max, axis=0)
    moved_marks = jnp.concatenate(local_before, axis=0) + jnp.concatenate(
        [marks[h : h + 1, 0:1] for h in range(heads) for _ in range(blocks)], axis=0
    )
    start_marks = jnp.maximum(moved_marks, local_marks)
    moved_scale = jnp.exp(moved_marks - start_marks)
    local_scale = jnp.exp(local_marks - start_marks)
    from_start = within + start_marks
    joined = jnp.maximum(largest, from_start)
    scales = jnp.concatenate(
        [jnp.exp(largest - joined), jnp.exp(from_start - joined)], axis=0
    ).T
    rows = heads * blocks

    for b in range(blocks):
        for h in range(heads):
            row = h * blocks + b
            start = (
                moved_scale[row : row + 1] * earlier[h * keys : (h + 1) * keys, :]
                + local_scale[row : row + 1] * carried[row]
            )
            start_high, start_low = split(start)
            query = query_ref[b * BLOCK : (b + 1) * BLOCK, h * keys : (h + 1) * keys]
            query = query * jnp.bfloat16(keys ** -0.5)
            cell = scales[:, row : row + 1] * intra[row] + scales[
                :, rows + row : rows + row + 1
            ] * (dot_f32(query, start_high) + dot_f32(query, start_low))
            norm = lax.rsqrt(jnp.mean(cell * cell, axis=-1, keepdims=True) + epsilon)
            gate = jax.nn.sigmoid(
                gate_ref[b * BLOCK : (b + 1) * BLOCK, h * wide : (h + 1) * wide].astype(jnp.float32)
            )
            mix[b * BLOCK : (b + 1) * BLOCK, h * wide : (h + 1) * wide] = (
                gate * cell * norm * head_scale_ref[:, h * wide : (h + 1) * wide]
            ).astype(jnp.bfloat16)
        for target in range(tp_size):
            if b == ((target + 1) * share - 1) // BLOCK:
                @pl.when(tp != target)
                def _(target=target):
                    mix_copy(tp, target).start()

    token_mix[:, pl.ds(pl.multiple_of(tp * columns, columns), columns)] = mix[
        pl.ds(pl.multiple_of(tp * share, share), share), :
    ]
    weight_copy.wait()
    for k in range(1, tp_size):
        mix_copy(lax.rem(tp + k, tp_size), tp).wait_recv()
    width = weights.shape[1]
    tile = 256

    def project(t, squares):
        where = pl.ds(pl.multiple_of(t * tile, tile), tile)
        middle = (
            residual_ref[:, where].astype(jnp.float32)
            + dot_f32(token_mix[...], weights[:, where])
        ).astype(jnp.bfloat16)
        middle_ref[:, where] = middle
        middle = middle.astype(jnp.float32)
        return squares + jnp.sum(middle * middle, axis=-1, keepdims=True)

    squares = lax.fori_loop(
        0, width // tile, project, jnp.zeros((share, 1), jnp.float32)
    )
    norm = lax.rsqrt(squares * (1.0 / width) + epsilon)

    def scale_rows(t, carry):
        where = pl.ds(pl.multiple_of(t * tile, tile), tile)
        normed_ref[:, where] = (
            middle_ref[:, where].astype(jnp.float32) * norm * norm_scale_ref[:, where]
        ).astype(jnp.bfloat16)
        return carry

    lax.fori_loop(0, width // tile, scale_rows, 0)

    def finish(k, carry):
        @pl.when(sp + k < n)
        def _():
            for copy in state_copies(sp, sp + k):
                copy.wait_send()

        return carry

    lax.fori_loop(1, n, finish, 0)
    for k in range(1, tp_size):
        mix_copy(tp, lax.rem(tp + k, tp_size)).wait_send()


def cell_call(heads, experts, slots, arrays):
    queries, values, residual, projection = arrays[0], arrays[2], arrays[8], arrays[9]
    n = lax.axis_size("sp")
    tp_size = lax.axis_size("tp")
    length = queries.shape[0]
    keys = queries.shape[1] // heads
    wide = values.shape[1] // heads
    rows = heads * (length // BLOCK)
    tokens, width = residual.shape
    note_rows = -(-2 * heads // 8) * 8
    vmem = pl.BlockSpec(memory_space=pltpu.VMEM)
    anywhere = pl.BlockSpec(memory_space=pl.ANY)
    dma = pltpu.SemaphoreType.DMA
    specs = [vmem] * len(arrays)
    specs[9] = anywhere
    return pl.pallas_call(
        functools.partial(cell_kernel, n, tp_size, heads, experts, slots),
        out_shape=(
            jax.ShapeDtypeStruct((tokens, width), jnp.bfloat16),
            jax.ShapeDtypeStruct((tokens, width), jnp.bfloat16),
            jax.ShapeDtypeStruct((8, tokens), jnp.float32),
        ),
        in_specs=specs,
        out_specs=(vmem, vmem, vmem),
        scratch_shapes=[
            pltpu.VMEM((heads * keys, wide), jnp.bfloat16),
            pltpu.VMEM((note_rows, wide), jnp.float32),
            pltpu.VMEM((n, heads * keys, wide), jnp.bfloat16),
            pltpu.VMEM((n, note_rows, wide), jnp.float32),
            pltpu.VMEM((rows, keys, wide), jnp.float32),
            pltpu.VMEM((rows, BLOCK, wide), jnp.float32),
            pltpu.VMEM((length, heads * wide), jnp.bfloat16),
            pltpu.VMEM((tokens, projection.shape[0]), jnp.bfloat16),
            pltpu.VMEM(projection.shape, jnp.bfloat16),
            dma((n,)), dma((n,)), dma((n,)), dma((n,)),
            dma((tp_size,)), dma((tp_size,)),
            dma(()),
        ],
        compiler_params=pltpu.CompilerParams(collective_id=0, has_side_effects=True),
    )(*arrays)


def expert_kernel(tp_size, chunks, tile,
                  normed_ref, middle_ref, notes_ref, gate_ref, up_ref, down_ref, out_ref,
                  notes, rows, sent, arrived, produced, returned, outcome,
                  activation, gate_w, up_w, down_w,
                  notes_send, notes_recv, rows_send, rows_recv, there_send, there_recv,
                  back_send, back_recv, weight_sems):
    sp = lax.axis_index("sp")
    tp = lax.axis_index("tp")
    lanes, part = rows.shape[2:]
    halves, members, slots, wide = sent.shape[1:]
    each = chunks // halves
    width = halves * wide
    hidden = gate_w.shape[1]
    sp_rows = members // tp_size
    plane = sp // sp_rows
    member = lax.rem(sp, sp_rows) * tp_size + tp
    last = PLANES - 1
    upper = plane >= PLANES // 2
    outward = jnp.where(upper, 1, -1)
    at_end = (plane == 0) | (plane == last)

    def place(to_plane, to_member):
        return dict(
            device_id={"sp": to_plane * sp_rows + to_member // tp_size,
                       "tp": lax.rem(to_member, tp_size)},
            device_id_type=MESH,
        )

    def beside(step):
        return lax.rem(plane + step + PLANES, PLANES)

    weight_copies = [
        pltpu.make_async_copy(source.at[0], target, weight_sems.at[k])
        for k, (source, target) in enumerate(
            ((gate_ref, gate_w), (up_ref, up_w), (down_ref, down_w))
        )
    ]
    for copy in weight_copies:
        copy.start()

    barrier = pltpu.get_barrier_semaphore()
    for k in range(1, members):
        pl.semaphore_signal(barrier, inc=1, **place(plane, lax.rem(member + k, members)))
    for k in range(1, PLANES):
        pl.semaphore_signal(barrier, inc=1, **place(beside(k), member))
    pl.semaphore_wait(barrier, members + PLANES - 2)

    def notes_copy(source, target):
        return pltpu.make_async_remote_copy(
            src_ref=notes_ref, dst_ref=notes.at[source],
            send_sem=notes_send.at[target], recv_sem=notes_recv.at[source],
            **place(target, member))

    def rows_copy(block, k, step, own=False):
        source = normed_ref.at[:, pl.ds(k * part, part)] if own else rows.at[block, k]
        return pltpu.make_async_remote_copy(
            src_ref=source, dst_ref=rows.at[block, k],
            send_sem=rows_send.at[(step + 1) // 2, block, k], recv_sem=rows_recv.at[block, k],
            **place(beside(step), member))

    def there(block, half, target):
        return pltpu.make_async_remote_copy(
            src_ref=sent.at[block, half, target], dst_ref=arrived.at[block, half, member],
            send_sem=there_send.at[block, half], recv_sem=there_recv.at[block, half],
            **place(plane, target))

    def back(block, half, target):
        return pltpu.make_async_remote_copy(
            src_ref=produced.at[block, half, target],
            dst_ref=returned.at[plane, half, member],
            send_sem=back_send.at[block, half], recv_sem=back_recv.at[plane, half],
            **place(block, target))

    def bytes_of(buffer, block, half, sem, count):
        span = buffer.at[block, half, pl.ds(0, count)]
        return pltpu.make_async_copy(span, span, sem.at[block, half])

    for k in range(1, PLANES):
        notes_copy(plane, beside(k)).start()
    for step in (1, -1):
        @pl.when((plane + step >= 0) & (plane + step <= last))
        def _(step=step):
            for k in range(chunks):
                rows_copy(plane, k, step, True).start()
    notes[plane] = notes_ref[...]
    for k in range(chunks):
        rows[plane, k] = normed_ref[:, k * part : (k + 1) * part]

    def matches(block, of_plane):
        slot = lax.broadcasted_iota(jnp.int32, (members * slots, lanes), 0)
        slot = (slot + of_plane * (members * slots)).astype(jnp.float32)
        return notes[block, 0:1, :] == slot, notes[block, 1:2, :] == slot

    def dispatch(block, half):
        first, second = matches(block, plane)
        pick = jnp.where(first | second, 1.0, 0.0).astype(jnp.bfloat16)
        for k in range(each):
            chosen = dot_f32(pick, rows[block, half * each + k]).astype(jnp.bfloat16)
            sent[block, half, :, :, k * part : (k + 1) * part] = chosen.reshape(
                members, slots, part
            )
        for i in range(1, members):
            there(block, half, lax.rem(member + i, members)).start()
        arrived[block, half, member] = sent[block, half, member]

    def take(block, half, forward):
        for k in range(half * each, (half + 1) * each):
            rows_copy(block, k, -1).wait_recv()
            if forward is not None:
                rows_copy(block, k, forward).start()
        dispatch(block, half)

    def give_back(block, half):
        for i in range(1, members):
            back(block, half, lax.rem(member + i, members)).start()
        back(block, half, member).start()

    def give_home():
        for half in range(halves):
            for i in range(1, members):
                back(plane, half, lax.rem(member + i, members)).start()
            returned[plane, half, member] = produced[plane, half, member]

    def give_late(block):
        for half in range(halves):
            give_back(block, half)

    def compute(block, send=True):
        for half in range(halves):
            bytes_of(arrived, block, half, there_recv, members - 1).wait()

        def hidden_tile(t, carry):
            columns = pl.ds(pl.multiple_of(t * tile, tile), tile)
            gate_part = up_part = 0.0
            for half in range(halves):
                tokens = arrived[block, half].reshape(members * slots, wide)
                span = slice(half * wide, (half + 1) * wide)
                gate_part = gate_part + dot_f32(tokens, gate_w[span, columns])
                up_part = up_part + dot_f32(tokens, up_w[span, columns])
            activation[:, columns] = (jax.nn.silu(gate_part) * up_part).astype(jnp.bfloat16)
            return carry

        lax.fori_loop(0, hidden // tile, hidden_tile, 0)
        for half in range(halves):
            def width_tile(t, carry):
                start = pl.multiple_of(t * tile, tile)
                result = dot_f32(
                    activation[...], down_w[:, pl.ds(half * wide + start, tile)]
                ).astype(jnp.bfloat16)
                produced[block, half, :, :, pl.ds(start, tile)] = result.reshape(
                    members, slots, tile
                )
                return carry

            lax.fori_loop(0, wide // tile, width_tile, 0)
            if send:
                give_back(block, half)


    def gather(of_plane, home=False):
        first, second = matches(plane, of_plane)
        spread = jnp.where(first, notes[plane, 2:3, :], 0.0) + jnp.where(
            second, notes[plane, 3:4, :], 0.0
        )
        high, low = split(spread.T)
        for half in range(halves):
            bytes_of(returned, of_plane, half, back_recv, members - 1 if home else members).wait()
            for k in range(each):
                share = returned[of_plane, half, :, :, k * part : (k + 1) * part].reshape(
                    members * slots, part
                )
                columns = slice(half * wide + k * part, half * wide + (k + 1) * part)
                before = middle_ref[:, columns].astype(jnp.float32) if home else outcome[:, columns]
                outcome[:, columns] = before + dot_f32(high, share) + dot_f32(low, share)

    for half in range(halves):
        dispatch(plane, half)
    for k in range(1, PLANES):
        notes_copy(beside(k), plane).wait_recv()

    @pl.when(at_end)
    def _():
        one, two, three = plane - outward, plane - 2 * outward, plane - 3 * outward
        take(one, 0, None)
        take(one, 1, None)
        for copy in weight_copies:
            copy.wait()
        compute(plane, False)
        compute(one)
        take(two, 0, None)
        take(two, 1, None)
        give_home()
        compute(two)
        take(three, 0, None)
        take(three, 1, None)
        compute(three)
        gather(plane, True)
        gather(one)
        gather(two)
        gather(three)

    @pl.when(jnp.logical_not(at_end))
    def _():
        inner, outer, far = plane - outward, plane + outward, plane - 2 * outward
        take(inner, 0, outward)
        take(outer, 0, -outward)
        take(inner, 1, outward)
        take(outer, 1, -outward)
        for copy in weight_copies:
            copy.wait()
        compute(plane, False)
        compute(inner)
        take(far, 0, outward)
        take(far, 1, outward)
        compute(outer)
        compute(far)
        give_home()
        gather(plane, True)
        gather(outer)
        gather(inner)
        gather(far)

    out_ref[...] = outcome[...].astype(jnp.bfloat16)
    for k in range(1, PLANES):
        notes_copy(plane, beside(k)).wait_send()

    def finish(block, carry):
        @pl.when((block <= plane) & (plane < last))
        def _():
            for k in range(chunks):
                rows_copy(block, k, 1).wait_send()

        @pl.when((block >= plane) & (plane > 0))
        def _():
            for k in range(chunks):
                rows_copy(block, k, -1).wait_send()

        for half in range(halves):
            bytes_of(sent, block, half, there_send, members - 1).wait()
            bytes_of(produced, block, half, back_send, members - 1).wait()

        @pl.when(block != plane)
        def _():
            for half in range(halves):
                bytes_of(produced, block, half, back_send, 1).wait()

        return carry

    lax.fori_loop(0, PLANES, finish, 0)


def expert_call(normed, middle, notes, gate, up, down, slots):
    tokens, width = normed.shape
    hidden = gate.shape[2]
    tp_size = lax.axis_size("tp")
    members = lax.axis_size("sp") * tp_size // PLANES
    chunks, halves = 4, 2
    part = width // chunks
    vmem = pl.BlockSpec(memory_space=pltpu.VMEM)
    anywhere = pl.BlockSpec(memory_space=pl.ANY)
    slotted = pltpu.VMEM((PLANES, halves, members, slots, width // halves), jnp.bfloat16)
    chunked = pltpu.VMEM((PLANES, chunks, tokens, part), jnp.bfloat16)
    dma = pltpu.SemaphoreType.DMA
    return pl.pallas_call(
        functools.partial(expert_kernel, tp_size, chunks, 256),
        out_shape=jax.ShapeDtypeStruct(middle.shape, jnp.bfloat16),
        in_specs=[vmem, vmem, vmem, anywhere, anywhere, anywhere],
        out_specs=vmem,
        scratch_shapes=[
            pltpu.VMEM((PLANES,) + notes.shape, jnp.float32),
            chunked,
            slotted,
            slotted,
            slotted,
            slotted,
            pltpu.VMEM((tokens, width), jnp.float32),
            pltpu.VMEM((members * slots, hidden), jnp.bfloat16),
            pltpu.VMEM((width, hidden), jnp.bfloat16),
            pltpu.VMEM((width, hidden), jnp.bfloat16),
            pltpu.VMEM((hidden, width), jnp.bfloat16),
            dma((PLANES,)),
            dma((PLANES,)),
            dma((2, PLANES, chunks)),
            dma((PLANES, chunks)),
            dma((PLANES, halves)),
            dma((PLANES, halves)),
            dma((PLANES, halves)),
            dma((PLANES, halves)),
            dma((3,)),
        ],
        compiler_params=pltpu.CompilerParams(collective_id=1, has_side_effects=True),
    )(normed, middle, notes, gate, up, down)


def shards(
    queries,
    keys,
    values,
    input_gate_log,
    forget_gate_logits,
    extra_decay_log,
    output_gate_logits,
    head_norm_scale,
    layer_residual_input,
    output_projection_weight,
    expert_norm_scale,
    routing_expert_index,
    routing_expert_weight,
    expert_gate_weight,
    expert_up_weight,
    expert_down_weight,
):
    sp_count = lax.axis_size("sp")
    tp_count = lax.axis_size("tp")
    devices = sp_count * tp_count
    local_experts = expert_gate_weight.shape[0]
    experts = local_experts * devices
    tok_count, model_width = layer_residual_input.shape
    slots = max(2, 2 * tok_count * TOP // experts)
    middle, normed, notes = cell_call(
        input_gate_log.shape[0], experts, slots,
        [
            queries, keys, values, input_gate_log, forget_gate_logits, extra_decay_log,
            output_gate_logits, head_norm_scale[None], layer_residual_input,
            output_projection_weight, expert_norm_scale[None], routing_expert_index.T,
            routing_expert_weight.T,
        ],
    )
    if (
        local_experts == 1
        and slots % 16 == 0
        and sp_count % PLANES == 0
        and model_width % 1024 == 0
    ):
        return expert_call(
            normed, middle, notes, expert_gate_weight, expert_up_weight, expert_down_weight, slots
        )
    slot_key = notes[:TOP].T.astype(jnp.int32).reshape(-1)
    matches = slot_key[None, :] == jnp.arange(experts * slots, dtype=jnp.int32)[:, None]
    pick = jnp.sum(
        matches.reshape(experts * slots, tok_count, TOP).astype(jnp.float32), axis=2
    ).astype(jnp.bfloat16)
    outgoing = (
        jnp.dot(pick, normed, preferred_element_type=jnp.float32)
        .astype(jnp.bfloat16)
        .reshape(experts, slots, model_width)
    )
    weight_high = lax.reduce_precision(routing_expert_weight, 8, 7)
    slot_pairs = slot_key.reshape(tok_count, TOP, 1)
    slot_range = jnp.arange(experts * slots, dtype=jnp.int32)

    def spread(weights):
        return jnp.sum(
            jnp.where(slot_pairs == slot_range, weights[:, :, None], 0.0), axis=1
        ).astype(jnp.bfloat16)

    high = spread(weight_high)
    low = spread(routing_expert_weight - weight_high)
    arrived = lax.all_to_all(outgoing, ("sp", "tp"), split_axis=0, concat_axis=0, tiled=True)
    grouped = arrived.reshape(devices, local_experts, arrived.shape[1], model_width)
    gate_part = jnp.einsum(
        "sxcd,xdf->sxcf", grouped, expert_gate_weight, preferred_element_type=jnp.float32
    )
    up_part = jnp.einsum(
        "sxcd,xdf->sxcf", grouped, expert_up_weight, preferred_element_type=jnp.float32
    )
    activation = (jax.nn.silu(gate_part) * up_part).astype(jnp.bfloat16)
    produced = jnp.einsum(
        "sxcf,xfd->sxcd", activation, expert_down_weight, preferred_element_type=jnp.float32
    ).astype(jnp.bfloat16)
    returned = lax.all_to_all(
        produced.reshape(arrived.shape), ("sp", "tp"), split_axis=0, concat_axis=0, tiled=True
    )
    returned = returned.reshape(experts * slots, model_width)
    expert_sum = jnp.dot(high, returned, preferred_element_type=jnp.float32) + jnp.dot(
        low, returned, preferred_element_type=jnp.float32
    )
    return (middle.astype(jnp.float32) + expert_sum).astype(jnp.bfloat16)


def solution(mesh):
    in_specs = (
        P("sp", "tp"),
        P("sp", "tp"),
        P("sp", "tp"),
        P("tp", "sp"),
        P("tp", "sp"),
        P("tp", "sp"),
        P("sp", "tp"),
        P("tp"),
        P(("sp", "tp"), None),
        P(),
        P(),
        P(("sp", "tp"), None),
        P(("sp", "tp"), None),
        P(("sp", "tp"), None, None),
        P(("sp", "tp"), None, None),
        P(("sp", "tp"), None, None),
    )
    out_specs = P(("sp", "tp"), None)
    return jax.shard_map(shards, mesh=mesh, in_specs=in_specs, out_specs=out_specs, check_vma=False)
```

time: 152 us -> 104 us (0.68)
  the two profiles are of different devices: /device:TPU:7 before, /device:TPU:0 now
where the time goes in v1:
time: 104 us
  Pallas kernels  102 us (98%)
  local copies, waits for them, and re-layouts  1.88 us (2%)
    pallas_call x1, Pallas kernels, expert_call(): pl.pallas_call(functools.partial(expert_kernel, tp_size, chunks, 256), ou...  84.6 us
    pallas_call x1, Pallas kernels, cell_call(): pl.pallas_call(functools.partial(cell_kernel, n, tp_size, heads, experts,...  17.1 us

profile of v1, /device:TPU:0, one launch (start us, length us, event | category | flops | bytes accessed | tf_op | source)
XLA Modules:
  0.0 103.6 jit_solution(3036665110409940185)
XLA Ops:
  0.0 17.1 %shard_map.154 = (bf16[128,2048]{1,0:T(8,128)(2,1)}, bf16[128,2048]{1,0:T(8,128)(2,1)}, f32[8,128]{1,0:T(8,128)}) custom-call(bf16[512,128]{1,0:T(8,128)(2,1)} %query_ref.1, bf16[512,128]{1,0:T(8,128)(2,1)} %key_ref.1, bf16[512,256]{1,0:T(8,128)(2,1)} %value_ref.1, f32[2,512]{1,0:T(2,128)} %input_ref.1, f32[2,512]{1,0:T(2,128)} %forget_ref.1, ...), custom_call_target="tpu_custom_call" | custom-call | tf_op jit(solution)/shard_map/pallas_call | solution.py:315
  17.1 84.6 %shard_map.155 = bf16[128,2048]{1,0:T(8,128)(2,1)} custom-call(bf16[128,2048]{1,0:T(8,128)(2,1)} %get-tuple-element.8.normed_ref, bf16[128,2048]{1,0:T(8,128)(2,1)} %get-tuple-element.9.middle_ref, f32[8,128]{1,0:T(8,128)} %get-tuple-element.10.notes_ref, bf16[1,2048,1024]{2,1,0:T(8,128)(2,1)} %gate_ref.3, bf16[1,2048,1024]{2,1,0:T(8,128)(2,1)} %up_ref.1, ...), custom_call_target="tpu_custom_call" | custom-call | tf_op jit(solution)/shard_map/pallas_call | solution.py:605
  101.7 1.9 %copy.18 = bf16[128,2048]{1,0:T(8,128)(2,1)} copy(bf16[128,2048]{1,0:T(8,128)(2,1)} %shard_map.155) | data formatting | bytes 1048576

commit v2 on v1

--- a/solution.py
+++ b/solution.py
@@ -57,12 +57,12 @@
     return jnp.concatenate(lines, axis=0)
 
 
-def cell_kernel(n, tp_size, heads, experts, slots,
-                query_ref, key_ref, value_ref, input_ref, forget_ref, extra_ref, gate_ref,
-                head_scale_ref, residual_ref, projection_ref, norm_scale_ref, index_ref, weight_ref,
-                middle_ref, normed_ref, notes_ref,
-                state, state_notes, got_state, got_notes, carried, intra, mix, token_mix, weights,
-                send_state, send_notes, recv_state, recv_notes, send_mix, recv_mix, weight_sem):
+def cell_body(n, tp_size, heads, experts, slots, inputs, scratch, barrier_count, announce, publish):
+    (query_ref, key_ref, value_ref, input_ref, forget_ref, extra_ref, gate_ref, head_scale_ref,
+     residual_ref, projection_ref, norm_scale_ref, index_ref, weight_ref) = inputs
+    (notes_ref, outcome, state, state_notes, got_state, got_notes, carried, intra, mix, token_mix,
+     weights, send_state, send_notes, recv_state, recv_notes, send_mix, recv_mix,
+     weight_sem) = scratch
     sp = lax.axis_index("sp")
     tp = lax.axis_index("tp")
     length = query_ref.shape[0]
@@ -75,18 +75,6 @@
     weight_copy = pltpu.make_async_copy(projection_ref, weights, weight_sem)
     weight_copy.start()
     barrier = pltpu.get_barrier_semaphore()
-
-    def greet_sp(k, carry):
-        pl.semaphore_signal(
-            barrier, inc=1, device_id={"sp": lax.rem(sp + k, n)}, device_id_type=MESH
-        )
-        return carry
-
-    lax.fori_loop(1, n, greet_sp, 0)
-    for k in range(1, tp_size):
-        pl.semaphore_signal(
-            barrier, inc=1, device_id={"tp": lax.rem(tp + k, tp_size)}, device_id_type=MESH
-        )
 
     def state_copies(source, target):
         kind = dict(device_id={"sp": target}, device_id_type=MESH)
@@ -152,12 +140,12 @@
         state[h * keys : (h + 1) * keys, :] = memory.astype(jnp.bfloat16)
         state_notes[h : h + 1, :] = jnp.broadcast_to(passed, (1, wide))
         state_notes[heads + h : heads + h + 1, :] = jnp.broadcast_to(high_mark, (1, wide))
-    pl.semaphore_wait(barrier, n + tp_size - 2)
+    pl.semaphore_wait(barrier, barrier_count)
 
     def send_on(k, carry):
-        @pl.when(sp + k < n)
+        @pl.when(sp + n - k < n)
         def _():
-            for copy in state_copies(sp, sp + k):
+            for copy in state_copies(sp, sp + n - k):
                 copy.start()
 
         return carry
@@ -165,6 +153,7 @@
     lax.fori_loop(1, n, send_on, 0)
 
     notes_ref[...] = route_notes(index_ref, weight_ref, experts, slots)
+    announce()
     causal = lax.broadcasted_iota(jnp.int32, (BLOCK, BLOCK), 0) >= lax.broadcasted_iota(
         jnp.int32, (BLOCK, BLOCK), 1
     )
@@ -258,7 +247,7 @@
     for k in range(1, tp_size):
         mix_copy(lax.rem(tp + k, tp_size), tp).wait_recv()
     width = weights.shape[1]
-    tile = 256
+    tile = 512
 
     def project(t, squares):
         where = pl.ds(pl.multiple_of(t * tile, tile), tile)
@@ -266,8 +255,8 @@
             residual_ref[:, where].astype(jnp.float32)
             + dot_f32(token_mix[...], weights[:, where])
         ).astype(jnp.bfloat16)
-        middle_ref[:, where] = middle
         middle = middle.astype(jnp.float32)
+        outcome[:, where] = middle
         return squares + jnp.sum(middle * middle, axis=-1, keepdims=True)
 
     squares = lax.fori_loop(
@@ -275,14 +264,7 @@
     )
     norm = lax.rsqrt(squares * (1.0 / width) + epsilon)
 
-    def scale_rows(t, carry):
-        where = pl.ds(pl.multiple_of(t * tile, tile), tile)
-        normed_ref[:, where] = (
-            middle_ref[:, where].astype(jnp.float32) * norm * norm_scale_ref[:, where]
-        ).astype(jnp.bfloat16)
-        return carry
-
-    lax.fori_loop(0, width // tile, scale_rows, 0)
+    publish(norm, norm_scale_ref)
 
     def finish(k, carry):
         @pl.when(sp + k < n)
@@ -297,19 +279,70 @@
         mix_copy(tp, lax.rem(tp + k, tp_size)).wait_send()
 
 
-def cell_call(heads, experts, slots, arrays):
-    queries, values, residual, projection = arrays[0], arrays[2], arrays[8], arrays[9]
-    n = lax.axis_size("sp")
-    tp_size = lax.axis_size("tp")
+def greet_sp(n):
+    sp = lax.axis_index("sp")
+    barrier = pltpu.get_barrier_semaphore()
+
+    def one(k, carry):
+        pl.semaphore_signal(
+            barrier, inc=1, device_id={"sp": lax.rem(sp + k, n)}, device_id_type=MESH
+        )
+        return carry
+
+    lax.fori_loop(1, n, one, 0)
+
+
+def cell_kernel(n, tp_size, heads, experts, slots, *refs):
+    inputs, (middle_ref, normed_ref, notes_ref), scratch = refs[:13], refs[13:16], refs[16:]
+    outcome = scratch[0]
+    tp = lax.axis_index("tp")
+    greet_sp(n)
+    for k in range(1, tp_size):
+        pl.semaphore_signal(
+            pltpu.get_barrier_semaphore(), inc=1,
+            device_id={"tp": lax.rem(tp + k, tp_size)}, device_id_type=MESH,
+        )
+
+    def publish(norm, norm_scale_ref):
+        middle_ref[...] = outcome[...].astype(jnp.bfloat16)
+        normed_ref[...] = (outcome[...] * norm * norm_scale_ref[...]).astype(jnp.bfloat16)
+
+    cell_body(n, tp_size, heads, experts, slots, inputs, (notes_ref,) + scratch,
+              n + tp_size - 2, lambda: None, publish)
+
+
+def cell_scratch(heads, n, tp_size, queries, values, residual, projection):
     length = queries.shape[0]
     keys = queries.shape[1] // heads
     wide = values.shape[1] // heads
     rows = heads * (length // BLOCK)
     tokens, width = residual.shape
     note_rows = -(-2 * heads // 8) * 8
+    dma = pltpu.SemaphoreType.DMA
+    return [
+        pltpu.VMEM((tokens, width), jnp.float32),
+        pltpu.VMEM((heads * keys, wide), jnp.bfloat16),
+        pltpu.VMEM((note_rows, wide), jnp.float32),
+        pltpu.VMEM((n, heads * keys, wide), jnp.bfloat16),
+        pltpu.VMEM((n, note_rows, wide), jnp.float32),
+        pltpu.VMEM((rows, keys, wide), jnp.float32),
+        pltpu.VMEM((rows, BLOCK, wide), jnp.float32),
+        pltpu.VMEM((length, heads * wide), jnp.bfloat16),
+        pltpu.VMEM((tokens, projection.shape[0]), jnp.bfloat16),
+        pltpu.VMEM(projection.shape, jnp.bfloat16),
+        dma((n,)), dma((n,)), dma((n,)), dma((n,)),
+        dma((tp_size,)), dma((tp_size,)),
+        dma(()),
+    ]
+
+
+def cell_call(heads, experts, slots, arrays):
+    queries, values, residual, projection = arrays[0], arrays[2], arrays[8], arrays[9]
+    n = lax.axis_size("sp")
+    tp_size = lax.axis_size("tp")
+    tokens, width = residual.shape
     vmem = pl.BlockSpec(memory_space=pltpu.VMEM)
     anywhere = pl.BlockSpec(memory_space=pl.ANY)
-    dma = pltpu.SemaphoreType.DMA
     specs = [vmem] * len(arrays)
     specs[9] = anywhere
     return pl.pallas_call(
@@ -321,30 +354,18 @@
         ),
         in_specs=specs,
         out_specs=(vmem, vmem, vmem),
-        scratch_shapes=[
-            pltpu.VMEM((heads * keys, wide), jnp.bfloat16),
-            pltpu.VMEM((note_rows, wide), jnp.float32),
-            pltpu.VMEM((n, heads * keys, wide), jnp.bfloat16),
-            pltpu.VMEM((n, note_rows, wide), jnp.float32),
-            pltpu.VMEM((rows, keys, wide), jnp.float32),
-            pltpu.VMEM((rows, BLOCK, wide), jnp.float32),
-            pltpu.VMEM((length, heads * wide), jnp.bfloat16),
-            pltpu.VMEM((tokens, projection.shape[0]), jnp.bfloat16),
-            pltpu.VMEM(projection.shape, jnp.bfloat16),
-            dma((n,)), dma((n,)), dma((n,)), dma((n,)),
-            dma((tp_size,)), dma((tp_size,)),
-            dma(()),
-        ],
+        scratch_shapes=cell_scratch(heads, n, tp_size, queries, values, residual, projection),
         compiler_params=pltpu.CompilerParams(collective_id=0, has_side_effects=True),
     )(*arrays)
 
 
-def expert_kernel(tp_size, chunks, tile,
-                  normed_ref, middle_ref, notes_ref, gate_ref, up_ref, down_ref, out_ref,
-                  notes, rows, sent, arrived, produced, returned, outcome,
-                  activation, gate_w, up_w, down_w,
-                  notes_send, notes_recv, rows_send, rows_recv, there_send, there_recv,
-                  back_send, back_recv, weight_sems):
+def layer_kernel(n, tp_size, heads, experts, chunks, tile, *refs):
+    inputs, (gate_ref, up_ref, down_ref), out_ref = refs[:13], refs[13:16], refs[16]
+    (notes, rows, sent, arrived, produced, returned, activation, gate_w, up_w, down_w,
+     notes_send, notes_recv, rows_send, rows_recv, there_send, there_recv,
+     back_send, back_recv, weight_sems) = refs[17:36]
+    cell_refs = refs[36:]
+    notes_ref, outcome = cell_refs[:2]
     sp = lax.axis_index("sp")
     tp = lax.axis_index("tp")
     lanes, part = rows.shape[2:]
@@ -376,15 +397,10 @@
             ((gate_ref, gate_w), (up_ref, up_w), (down_ref, down_w))
         )
     ]
-    for copy in weight_copies:
-        copy.start()
-
     barrier = pltpu.get_barrier_semaphore()
+    greet_sp(n)
     for k in range(1, members):
         pl.semaphore_signal(barrier, inc=1, **place(plane, lax.rem(member + k, members)))
-    for k in range(1, PLANES):
-        pl.semaphore_signal(barrier, inc=1, **place(beside(k), member))
-    pl.semaphore_wait(barrier, members + PLANES - 2)
 
     def notes_copy(source, target):
         return pltpu.make_async_remote_copy(
@@ -392,10 +408,9 @@
             send_sem=notes_send.at[target], recv_sem=notes_recv.at[source],
             **place(target, member))
 
-    def rows_copy(block, k, step, own=False):
-        source = normed_ref.at[:, pl.ds(k * part, part)] if own else rows.at[block, k]
+    def rows_copy(block, k, step):
         return pltpu.make_async_remote_copy(
-            src_ref=source, dst_ref=rows.at[block, k],
+            src_ref=rows.at[block, k], dst_ref=rows.at[block, k],
             send_sem=rows_send.at[(step + 1) // 2, block, k], recv_sem=rows_recv.at[block, k],
             **place(beside(step), member))
 
@@ -416,16 +431,31 @@
         span = buffer.at[block, half, pl.ds(0, count)]
         return pltpu.make_async_copy(span, span, sem.at[block, half])
 
-    for k in range(1, PLANES):
-        notes_copy(plane, beside(k)).start()
-    for step in (1, -1):
-        @pl.when((plane + step >= 0) & (plane + step <= last))
-        def _(step=step):
-            for k in range(chunks):
-                rows_copy(plane, k, step, True).start()
-    notes[plane] = notes_ref[...]
-    for k in range(chunks):
-        rows[plane, k] = normed_ref[:, k * part : (k + 1) * part]
+    def announce():
+        for k in range(1, PLANES):
+            notes_copy(plane, beside(k)).start()
+        notes[plane] = notes_ref[...]
+        for copy in weight_copies:
+            copy.start()
+
+    def send_rows(k):
+        for step in (1, -1):
+            @pl.when((plane + step >= 0) & (plane + step <= last))
+            def _(step=step):
+                rows_copy(plane, k, step).start()
+
+    def publish(norm, norm_scale_ref):
+        for k in range(chunks):
+            columns = slice(k * part, (k + 1) * part)
+            rows[plane, k] = (outcome[:, columns] * norm * norm_scale_ref[:, columns]).astype(
+                jnp.bfloat16
+            )
+            if k > 0:
+                send_rows(k - 1)
+        send_rows(chunks - 1)
+
+    cell_body(n, tp_size, heads, experts, slots, inputs, cell_refs,
+              n + members - 2, announce, publish)
 
     def matches(block, of_plane):
         slot = lax.broadcasted_iota(jnp.int32, (members * slots, lanes), 0)
@@ -511,8 +541,7 @@
                     members * slots, part
                 )
                 columns = slice(half * wide + k * part, half * wide + (k + 1) * part)
-                before = middle_ref[:, columns].astype(jnp.float32) if home else outcome[:, columns]
-                outcome[:, columns] = before + dot_f32(high, share) + dot_f32(low, share)
+                outcome[:, columns] += dot_f32(high, share) + dot_f32(low, share)
 
     for half in range(halves):
         dispatch(plane, half)
@@ -590,31 +619,32 @@
     lax.fori_loop(0, PLANES, finish, 0)
 
 
-def expert_call(normed, middle, notes, gate, up, down, slots):
-    tokens, width = normed.shape
+def layer_call(heads, experts, slots, arrays, gate, up, down):
+    queries, values, residual, projection = arrays[0], arrays[2], arrays[8], arrays[9]
+    tokens, width = residual.shape
     hidden = gate.shape[2]
+    n = lax.axis_size("sp")
     tp_size = lax.axis_size("tp")
-    members = lax.axis_size("sp") * tp_size // PLANES
+    members = n * tp_size // PLANES
     chunks, halves = 4, 2
-    part = width // chunks
     vmem = pl.BlockSpec(memory_space=pltpu.VMEM)
     anywhere = pl.BlockSpec(memory_space=pl.ANY)
     slotted = pltpu.VMEM((PLANES, halves, members, slots, width // halves), jnp.bfloat16)
-    chunked = pltpu.VMEM((PLANES, chunks, tokens, part), jnp.bfloat16)
     dma = pltpu.SemaphoreType.DMA
+    specs = [vmem] * len(arrays) + [anywhere] * 3
+    specs[9] = anywhere
     return pl.pallas_call(
-        functools.partial(expert_kernel, tp_size, chunks, 256),
-        out_shape=jax.ShapeDtypeStruct(middle.shape, jnp.bfloat16),
-        in_specs=[vmem, vmem, vmem, anywhere, anywhere, anywhere],
+        functools.partial(layer_kernel, n, tp_size, heads, experts, chunks, 256),
+        out_shape=jax.ShapeDtypeStruct(residual.shape, jnp.bfloat16),
+        in_specs=specs,
         out_specs=vmem,
         scratch_shapes=[
-            pltpu.VMEM((PLANES,) + notes.shape, jnp.float32),
-            chunked,
+            pltpu.VMEM((PLANES, 8, tokens), jnp.float32),
+            pltpu.VMEM((PLANES, chunks, tokens, width // chunks), jnp.bfloat16),
             slotted,
             slotted,
             slotted,
             slotted,
-            pltpu.VMEM((tokens, width), jnp.float32),
             pltpu.VMEM((members * slots, hidden), jnp.bfloat16),
             pltpu.VMEM((width, hidden), jnp.bfloat16),
             pltpu.VMEM((width, hidden), jnp.bfloat16),
@@ -628,9 +658,11 @@
             dma((PLANES, halves)),
             dma((PLANES, halves)),
             dma((3,)),
-        ],
+            pltpu.VMEM((8, tokens), jnp.float32),
+        ]
+        + cell_scratch(heads, n, tp_size, queries, values, residual, projection),
         compiler_params=pltpu.CompilerParams(collective_id=1, has_side_effects=True),
-    )(normed, middle, notes, gate, up, down)
+    )(*arrays, gate, up, down)
 
 
 def shards(
@@ -658,24 +690,24 @@
     experts = local_experts * devices
     tok_count, model_width = layer_residual_input.shape
     slots = max(2, 2 * tok_count * TOP // experts)
-    middle, normed, notes = cell_call(
-        input_gate_log.shape[0], experts, slots,
-        [
-            queries, keys, values, input_gate_log, forget_gate_logits, extra_decay_log,
-            output_gate_logits, head_norm_scale[None], layer_residual_input,
-            output_projection_weight, expert_norm_scale[None], routing_expert_index.T,
-            routing_expert_weight.T,
-        ],
-    )
+    heads = input_gate_log.shape[0]
+    arrays = [
+        queries, keys, values, input_gate_log, forget_gate_logits, extra_decay_log,
+        output_gate_logits, head_norm_scale[None], layer_residual_input,
+        output_projection_weight, expert_norm_scale[None], routing_expert_index.T,
+        routing_expert_weight.T,
+    ]
     if (
         local_experts == 1
         and slots % 16 == 0
         and sp_count % PLANES == 0
         and model_width % 1024 == 0
     ):
-        return expert_call(
-            normed, middle, notes, expert_gate_weight, expert_up_weight, expert_down_weight, slots
+        return layer_call(
+            heads, experts, slots, arrays,
+            expert_gate_weight, expert_up_weight, expert_down_weight,
         )
+    middle, normed, notes = cell_call(heads, experts, slots, arrays)
     slot_key = notes[:TOP].T.astype(jnp.int32).reshape(-1)
     matches = slot_key[None, :] == jnp.arange(experts * slots, dtype=jnp.int32)[:, None]
     pick = jnp.sum(

time: 104 us -> 101 us (0.971)
  Pallas kernels: 102 us -> 99 us
    pallas_call x2 -> x1, Pallas kernels: 102 us -> 99 us  [layer_call(): pl.pallas_call(functools.partial(layer_kernel, n, tp_size, heads, experts...]
where the time goes in v2:
time: 101 us
  Pallas kernels  99 us (98%)
  local copies, waits for them, and re-layouts  1.88 us (2%)
    pallas_call x1, Pallas kernels, layer_call(): pl.pallas_call(functools.partial(layer_kernel, n, tp_size, heads, experts...  99 us

profile of v2, /device:TPU:0, one launch (start us, length us, event | category | flops | bytes accessed | tf_op | source)
XLA Modules:
  0.0 100.9 jit_solution(12407528354651019367)
XLA Ops:
  0.0 99.0 %shard_map.154 = bf16[128,2048]{1,0:T(8,128)(2,1)} custom-call(bf16[512,128]{1,0:T(8,128)(2,1)} %refs_0_.1, bf16[512,128]{1,0:T(8,128)(2,1)} %refs_1_.1, bf16[512,256]{1,0:T(8,128)(2,1)} %refs_2_.1, f32[2,512]{1,0:T(2,128)} %refs_3_.1, f32[2,512]{1,0:T(2,128)} %refs_4_.1, f32[2,512]{1,0:T(2,128)} %refs_5_.1, bf16[512,256]{1,0:T(8,128)(2,1)} %refs_6_.1, ...), custom_call_target="tpu_custom_call" | custom-call | tf_op jit(solution)/shard_map/pallas_call | solution.py:636
  99.0 1.9 %copy.18 = bf16[128,2048]{1,0:T(8,128)(2,1)} copy(bf16[128,2048]{1,0:T(8,128)(2,1)} %shard_map.154) | data formatting | bytes 1048576

commit v3 on v2

--- a/solution.py
+++ b/solution.py
@@ -57,7 +57,7 @@
     return jnp.concatenate(lines, axis=0)
 
 
-def cell_body(n, tp_size, heads, experts, slots, inputs, scratch, barrier_count, announce, publish):
+def cell_body(n, tp_size, heads, experts, slots, inputs, scratch, barrier_count, announce, settled, mixed, publish):
     (query_ref, key_ref, value_ref, input_ref, forget_ref, extra_ref, gate_ref, head_scale_ref,
      residual_ref, projection_ref, norm_scale_ref, index_ref, weight_ref) = inputs
     (notes_ref, outcome, state, state_notes, got_state, got_notes, carried, intra, mix, token_mix,
@@ -200,6 +200,7 @@
         (jnp.zeros((heads * keys, wide), jnp.float32), jnp.zeros((heads, wide), jnp.float32)),
     )
 
+    settled()
     local_marks = jnp.concatenate(local_max, axis=0)
     moved_marks = jnp.concatenate(local_before, axis=0) + jnp.concatenate(
         [marks[h : h + 1, 0:1] for h in range(heads) for _ in range(blocks)], axis=0
@@ -246,6 +247,7 @@
     weight_copy.wait()
     for k in range(1, tp_size):
         mix_copy(lax.rem(tp + k, tp_size), tp).wait_recv()
+    mixed()
     width = weights.shape[1]
     tile = 512
 
@@ -308,7 +310,7 @@
         normed_ref[...] = (outcome[...] * norm * norm_scale_ref[...]).astype(jnp.bfloat16)
 
     cell_body(n, tp_size, heads, experts, slots, inputs, (notes_ref,) + scratch,
-              n + tp_size - 2, lambda: None, publish)
+              n + tp_size - 2, lambda: None, lambda: None, lambda: None, publish)
 
 
 def cell_scratch(heads, n, tp_size, queries, values, residual, projection):
@@ -363,9 +365,12 @@
     inputs, (gate_ref, up_ref, down_ref), out_ref = refs[:13], refs[13:16], refs[16]
     (notes, rows, sent, arrived, produced, returned, activation, gate_w, up_w, down_w,
      notes_send, notes_recv, rows_send, rows_recv, there_send, there_recv,
-     back_send, back_recv, weight_sems) = refs[17:36]
-    cell_refs = refs[36:]
+     back_send, back_recv, weight_sems, residual_in, mix_in, residual_send, residual_recv,
+     mix_send, mix_recv) = refs[17:42]
+    cell_refs = refs[42:]
     notes_ref, outcome = cell_refs[:2]
+    token_mix, projection = cell_refs[9:11]
+    residual_ref, norm_scale = inputs[8], inputs[10]
     sp = lax.axis_index("sp")
     tp = lax.axis_index("tp")
     lanes, part = rows.shape[2:]
@@ -414,6 +419,24 @@
             send_sem=rows_send.at[(step + 1) // 2, block, k], recv_sem=rows_recv.at[block, k],
             **place(beside(step), member))
 
+    def residual_copy(k, step):
+        side = (1 - step) // 2
+        return pltpu.make_async_remote_copy(
+            src_ref=residual_ref.at[:, pl.ds(k * part, part)], dst_ref=residual_in.at[side, k],
+            send_sem=residual_send.at[side, k], recv_sem=residual_recv.at[side, k],
+            **place(beside(step), member))
+
+    def mix_copy(step):
+        side = (1 - step) // 2
+        return pltpu.make_async_remote_copy(
+            src_ref=token_mix, dst_ref=mix_in.at[side],
+            send_sem=mix_send.at[side], recv_sem=mix_recv.at[side],
+            **place(beside(step), member))
+
+    def to_neighbours(run):
+        for step in (1, -1):
+            pl.when((plane + step >= 0) & (plane + step <= last))(functools.partial(run, step))
+
     def there(block, half, target):
         return pltpu.make_async_remote_copy(
             src_ref=sent.at[block, half, target], dst_ref=arrived.at[block, half, member],
@@ -434,15 +457,20 @@
     def announce():
         for k in range(1, PLANES):
             notes_copy(plane, beside(k)).start()
+
         notes[plane] = notes_ref[...]
         for copy in weight_copies:
             copy.start()
 
-    def send_rows(k):
-        for step in (1, -1):
-            @pl.when((plane + step >= 0) & (plane + step <= last))
-            def _(step=step):
-                rows_copy(plane, k, step).start()
+    def settled():
+        def send_residual(step):
+            for k in range(chunks):
+                residual_copy(k, step).start()
+
+        to_neighbours(send_residual)
+
+    def mixed():
+        to_neighbours(lambda step: mix_copy(step).start())
 
     def publish(norm, norm_scale_ref):
         for k in range(chunks):
@@ -450,12 +478,9 @@
             rows[plane, k] = (outcome[:, columns] * norm * norm_scale_ref[:, columns]).astype(
                 jnp.bfloat16
             )
-            if k > 0:
-                send_rows(k - 1)
-        send_rows(chunks - 1)
 
     cell_body(n, tp_size, heads, experts, slots, inputs, cell_refs,
-              n + members - 2, announce, publish)
+              n + members - 2, announce, settled, mixed, publish)
 
     def matches(block, of_plane):
         slot = lax.broadcasted_iota(jnp.int32, (members * slots, lanes), 0)
@@ -474,6 +499,31 @@
             there(block, half, lax.rem(member + i, members)).start()
         arrived[block, half, member] = sent[block, half, member]
 
+    def rebuild(block, side, forward):
+        mix_copy(1 - 2 * side).wait_recv()
+        squares = jnp.zeros((lanes, 1), jnp.float32)
+        for k in range(chunks):
+            residual_copy(k, 1 - 2 * side).wait_recv()
+            columns = slice(k * part, (k + 1) * part)
+            middle = (
+                residual_in[side, k].astype(jnp.float32)
+                + dot_f32(mix_in[side], projection[:, columns])
+            ).astype(jnp.bfloat16)
+            rows[block, k] = middle
+            middle = middle.astype(jnp.float32)
+            squares = squares + jnp.sum(middle * middle, axis=-1, keepdims=True)
+        norm = lax.rsqrt(squares * (1.0 / width) + epsilon)
+        for k in range(chunks):
+            columns = slice(k * part, (k + 1) * part)
+            rows[block, k] = (
+                rows[block, k].astype(jnp.float32) * norm * norm_scale[:, columns]
+            ).astype(jnp.bfloat16)
+        for half in range(halves):
+            dispatch(block, half)
+            if forward is not None:
+                for k in range(half * each, (half + 1) * each):
+                    rows_copy(block, k, forward).start()
+
     def take(block, half, forward):
         for k in range(half * each, (half + 1) * each):
             rows_copy(block, k, -1).wait_recv()
@@ -482,9 +532,9 @@
         dispatch(block, half)
 
     def give_back(block, half):
+        back(block, half, member).start()
         for i in range(1, members):
             back(block, half, lax.rem(member + i, members)).start()
-        back(block, half, member).start()
 
     def give_home():
         for half in range(halves):
@@ -551,8 +601,7 @@
     @pl.when(at_end)
     def _():
         one, two, three = plane - outward, plane - 2 * outward, plane - 3 * outward
-        take(one, 0, None)
-        take(one, 1, None)
+        rebuild(one, jnp.where(upper, 0, 1), None)
         for copy in weight_copies:
             copy.wait()
         compute(plane, False)
@@ -572,16 +621,15 @@
     @pl.when(jnp.logical_not(at_end))
     def _():
         inner, outer, far = plane - outward, plane + outward, plane - 2 * outward
-        take(inner, 0, outward)
-        take(outer, 0, -outward)
-        take(inner, 1, outward)
-        take(outer, 1, -outward)
+        rebuild(inner, jnp.where(upper, 0, 1), outward)
+        rebuild(outer, jnp.where(upper, 1, 0), -outward)
         for copy in weight_copies:
             copy.wait()
         compute(plane, False)
-        compute(inner)
+        compute(inner, False)
         take(far, 0, outward)
         take(far, 1, outward)
+        give_late(inner)
         compute(outer)
         compute(far)
         give_home()
@@ -594,13 +642,20 @@
     for k in range(1, PLANES):
         notes_copy(plane, beside(k)).wait_send()
 
+    def sent_early(step):
+        mix_copy(step).wait_send()
+        for k in range(chunks):
+            residual_copy(k, step).wait_send()
+
+    to_neighbours(sent_early)
+
     def finish(block, carry):
-        @pl.when((block <= plane) & (plane < last))
+        @pl.when((block < plane) & (plane < last))
         def _():
             for k in range(chunks):
                 rows_copy(block, k, 1).wait_send()
 
-        @pl.when((block >= plane) & (plane > 0))
+        @pl.when((block > plane) & (plane > 0))
         def _():
             for k in range(chunks):
                 rows_copy(block, k, -1).wait_send()
@@ -634,7 +689,7 @@
     specs = [vmem] * len(arrays) + [anywhere] * 3
     specs[9] = anywhere
     return pl.pallas_call(
-        functools.partial(layer_kernel, n, tp_size, heads, experts, chunks, 256),
+        functools.partial(layer_kernel, n, tp_size, heads, experts, chunks, 512),
         out_shape=jax.ShapeDtypeStruct(residual.shape, jnp.bfloat16),
         in_specs=specs,
         out_specs=vmem,
@@ -658,6 +713,12 @@
             dma((PLANES, halves)),
             dma((PLANES, halves)),
             dma((3,)),
+            pltpu.VMEM((2, chunks, tokens, width // chunks), jnp.bfloat16),
+            pltpu.VMEM((2, tokens, projection.shape[0]), jnp.bfloat16),
+            dma((2, chunks)),
+            dma((2, chunks)),
+            dma((2,)),
+            dma((2,)),
             pltpu.VMEM((8, tokens), jnp.float32),
         ]
         + cell_scratch(heads, n, tp_size, queries, values, residual, projection),

time: 101 us -> 98.8 us (0.978)
  Pallas kernels: 99 us -> 96.7 us
    pallas_call x1, Pallas kernels: 99 us -> 96.7 us  [layer_call(): pl.pallas_call(functools.partial(layer_kernel, n, tp_size, heads, experts...]
where the time goes in v3:
time: 98.8 us; the launch traced here: 98.6 us
  Pallas kernels  96.7 us (98%)
  local copies, waits for them, and re-layouts  1.88 us (2%)
    pallas_call x1, Pallas kernels, layer_call(): pl.pallas_call(functools.partial(layer_kernel, n, tp_size, heads, experts...  96.7 us

profile of v3, /device:TPU:0, one launch (start us, length us, event | category | flops | bytes accessed | tf_op | source)
XLA Modules:
  0.0 98.6 jit_solution(2443488538845381989)
XLA Ops:
  0.0 96.7 %shard_map.154 = bf16[128,2048]{1,0:T(8,128)(2,1)} custom-call(bf16[512,128]{1,0:T(8,128)(2,1)} %refs_0_.1, bf16[512,128]{1,0:T(8,128)(2,1)} %refs_1_.1, bf16[512,256]{1,0:T(8,128)(2,1)} %refs_2_.1, f32[2,512]{1,0:T(2,128)} %refs_3_.1, f32[2,512]{1,0:T(2,128)} %refs_4_.1, f32[2,512]{1,0:T(2,128)} %refs_5_.1, bf16[512,256]{1,0:T(8,128)(2,1)} %refs_6_.1, ...), custom_call_target="tpu_custom_call" | custom-call | tf_op jit(solution)/shard_map/pallas_call | solution.py:691
  96.7 1.9 %copy.18 = bf16[128,2048]{1,0:T(8,128)(2,1)} copy(bf16[128,2048]{1,0:T(8,128)(2,1)} %shard_map.154) | data formatting | bytes 1048576
